TPU v7x, 32 devices: a whole 2x2x4 slice. The times are simulated.
32 devices in a mesh: sp: 8 (over z, y), tp: 4 (over x, core).
Axes of the slice: x: 2, y: 2, z: 4, core: 2. Of those that a mesh axis runs over, the one named last changes fastest.
Arguments:
- tokens: bfloat16 [3072, 2048], P('sp'), may hold values from -6 to 6
- in_gain: float32 [2048], replicated, may hold values from 0.1 to 1.9
- query_weight: bfloat16 [2048, 1024], P(None, 'tp'), may hold values from -0.125 to 0.125
- key_weight: bfloat16 [2048, 1024], P(None, 'tp'), may hold values from -0.125 to 0.125
- value_weight: bfloat16 [2048, 2048], P(None, 'tp'), may hold values from -0.125 to 0.125
- gate_weight: bfloat16 [2048, 2048], P(None, 'tp'), may hold values from -0.125 to 0.125
- decay_down: bfloat16 [2048, 32], replicated, may hold values from -0.125 to 0.125
- decay_up: bfloat16 [32, 1024], replicated, may hold values from -1 to 1
- decay_offset: float32 [1024], P('tp')
- decay_extra: float32 [3072, 1024], P('sp', 'tp'), may hold values from -2 to 0, as said below
- head_gain: float32 [2048], P('tp'), may hold values from 0.1 to 1.9
- out_weight: bfloat16 [2048, 2048], P(None, 'tp'), may hold values from -4 to 4
- out_gain: float32 [2048], P('tp'), may hold values from 0.1 to 1.9
Outputs:
- layer_output: bfloat16 [3072, 2048], P('sp', 'tp')
Inputs may be any that keep to these rules, and one draw needn't show every extreme that they name: `decay_extra`: never positive.
All inputs are finite; a program needn't handle non-finite values.
Results may differ from a plain program's by a relative error of at most 0.015.
Values may be sent and summed in bfloat16 or wider, within the bound.
No kernel may reach another device: no remote copies, remote signals or barrier semaphores. Data moves between devices by JAX's collectives and lax.ppermute only.
A program may use at most 64 MiB of HBM per device.

v0:
```python
import jax
import jax.numpy as jnp
from jax import lax
from jax.sharding import PartitionSpec as P

D = 2048
QUERY_FEATURES = 128
DV = 256
BLOCK = 64


norm_eps = 1e-06
decay_temper = 16.0
highest = lax.Precision.HIGHEST


def entering(part, axis, combine, identity):
    place = lax.axis_index(axis)
    gathered = jax.tree.map(lambda a: lax.all_gather(a, axis), part)
    state = jax.tree.map(lambda a, e: jnp.zeros_like(a) + jnp.asarray(e, a.dtype), part, identity)

    def one(lap, state):
        return combine(
            state, jax.tree.map(lambda a: lax.dynamic_index_in_dim(a, lap, 0, False), gathered)
        )

    return lax.fori_loop(0, place, one, state)


def combine_states(earlier, latter):
    decay_first, state_first = earlier
    decay_second, state_second = latter
    return (decay_first * decay_second, decay_second[:, :, None] * state_first + state_second)


def block_pass(query_heads, key_heads, value_heads, decay_heads, state_start):
    row_count = query_heads.shape[0]
    block_count = row_count // BLOCK
    causal_mask = jnp.arange(BLOCK)[:, None] >= jnp.arange(BLOCK)[None, :]

    def to_blocks(values):
        return values.reshape(block_count, BLOCK, values.shape[1], values.shape[2])

    def block_step(carry_state, inputs):
        query_block, key_block, value_block, decay_block = inputs
        cumulative = jnp.cumsum(decay_block, axis=0)
        closing = cumulative[-1]
        query_inner = query_block * jnp.exp(cumulative)
        key_inner = key_block * jnp.exp(-cumulative)
        scores = jnp.einsum("chd,shd->hcs", query_inner, key_inner, precision=highest)
        scores = jnp.where(causal_mask[None], scores, 0.0)
        output = jnp.einsum("hcs,she->che", scores, value_block, precision=highest)
        output = output + jnp.einsum("chd,hde->che", query_inner, carry_state, precision=highest)
        key_closing = key_block * jnp.exp(closing[None] - cumulative)
        carry_state = carry_state * jnp.exp(closing)[:, :, None] + jnp.einsum(
            "chd,che->hde", key_closing, value_block, precision=highest
        )
        return (carry_state, output)

    state_end, outputs = lax.scan(
        block_step,
        state_start,
        (
            to_blocks(query_heads),
            to_blocks(key_heads),
            to_blocks(value_heads),
            to_blocks(decay_heads),
        ),
    )
    return (state_end, outputs.reshape(row_count, outputs.shape[2], outputs.shape[3]))


def link_scan(device_decay, local_state):
    decay_in, state_in = entering(
        (device_decay, local_state),
        "sp",
        combine_states,
        (jnp.ones_like(device_decay), jnp.zeros_like(local_state)),
    )
    return state_in


def carry_heads(query_heads, key_heads, value_heads, decay_heads, link_chain):
    empty_state = jnp.zeros((query_heads.shape[1], QUERY_FEATURES, DV), jnp.float32)
    cumulative = jnp.cumsum(decay_heads, axis=0)
    local_state, local_output = block_pass(
        query_heads, key_heads, value_heads, decay_heads, empty_state
    )
    device_decay = jnp.exp(jnp.sum(decay_heads, axis=0))
    carried = link_chain(device_decay, local_state)
    result = local_output + jnp.einsum(
        "thd,hde->the", query_heads * jnp.exp(cumulative), carried, precision=highest
    )
    return result


def local(
    tokens,
    in_gain,
    query_weight,
    key_weight,
    value_weight,
    gate_weight,
    decay_down,
    decay_up,
    decay_offset,
    decay_extra,
    head_gain,
    out_weight,
    out_gain,
):
    row_count = tokens.shape[0]
    head_count = query_weight.shape[1] // QUERY_FEATURES
    tokens_wide = tokens.astype(jnp.float32)
    normed = (
        tokens_wide
        * lax.rsqrt(jnp.mean(tokens_wide * tokens_wide, axis=1, keepdims=True) + norm_eps)
        * in_gain
    ).astype(jnp.bfloat16)

    def project(weight):
        return jnp.dot(normed, weight, preferred_element_type=jnp.float32).astype(jnp.bfloat16)

    query_rows = project(query_weight)
    key_rows = project(key_weight)
    value_rows = project(value_weight)
    gate_rows = project(gate_weight)
    low_rank = project(decay_down)
    channel_count = decay_offset.shape[0]
    up_columns = lax.dynamic_slice_in_dim(
        decay_up, lax.axis_index("tp") * channel_count, channel_count, 1
    )
    logits = jnp.dot(low_rank, up_columns, preferred_element_type=jnp.float32)
    log_decay = jax.nn.log_sigmoid(logits + decay_offset) / decay_temper + decay_extra
    query_heads = query_rows.astype(jnp.float32).reshape(row_count, head_count, QUERY_FEATURES)
    key_heads = key_rows.astype(jnp.float32).reshape(row_count, head_count, QUERY_FEATURES)
    value_heads = value_rows.astype(jnp.float32).reshape(row_count, head_count, DV)
    decay_heads = log_decay.reshape(row_count, head_count, QUERY_FEATURES)
    attended = carry_heads(query_heads, key_heads, value_heads, decay_heads, link_scan)
    scaled = (
        attended
        * lax.rsqrt(jnp.mean(attended * attended, axis=2, keepdims=True) + norm_eps)
        * head_gain.reshape(head_count, DV)
    )
    gated = (
        scaled.reshape(row_count, head_count * DV) * jax.nn.silu(gate_rows.astype(jnp.float32))
    ).astype(jnp.bfloat16)
    mixed = jnp.dot(
        lax.all_gather(gated, "tp", axis=1, tiled=True),
        out_weight,
        preferred_element_type=jnp.float32,
    )
    squares = lax.psum(jnp.sum(mixed * mixed, axis=1), "tp")
    result = mixed * lax.rsqrt(squares[:, None] / D + norm_eps) * out_gain
    return result.astype(jnp.bfloat16)


def solution(mesh):
    placed = (
        P("sp", None),
        P(),
        P(None, "tp"),
        P(None, "tp"),
        P(None, "tp"),
        P(None, "tp"),
        P(),
        P(),
        P("tp"),
        P("sp", "tp"),
        P("tp"),
        P(None, "tp"),
        P("tp"),
    )
    return jax.shard_map(
        local, mesh=mesh, in_specs=placed, out_specs=P("sp", "tp"), check_vma=False
    )
```

profile of v0, /device:TPU:0, one launch (start us, length us, event | category | flops | bytes accessed | tf_op | source)
XLA Modules:
  0.0 149.7 jit_solution(6956503692811085713)
XLA Ops:
  6.5 1.9 %fusion.18 = f32[384]{0:T(512)S(1)} fusion(bf16[384,2048]{1,0:T(8,128)(2,1)} %param.17), kind=kLoop, calls=%fused_computation.32 | loop fusion | flops 2358912 | bytes 1574400 | tf_op jit(solution)/shard_map/reduce_sum | solution.py:117
  8.5 2.6 %fusion.25 = f32[384,256]{0,1:T(8,128)S(1)} fusion(bf16[2048,256]{1,0:T(8,128)(2,1)} %param.19, bf16[384,2048]{1,0:T(8,128)(2,1)} %param.17, f32[2048]{0:T(1024)} %param.18, f32[384]{0:T(512)S(1)} %add_rsqrt_fusion.2), kind=kOutput, calls=%fused_computation.45 | convolution fusion | flops 405995520 | bytes 3024384 | tf_op jit(solution)/shard_map/dot_general | solution.py:122
  12.2 2.4 %fusion.26 = f32[384,256]{1,0:T(8,128)S(1)} fusion(bf16[2048,256]{1,0:T(8,128)(2,1)} %param.20, bf16[384,2048]{1,0:T(8,128)(2,1)} %param.17, f32[2048]{0:T(1024)S(1)} %copy-done.6, f32[384]{0:T(512)S(1)} %add_rsqrt_fusion.2), kind=kOutput, calls=%fused_computation.47 | convolution fusion | flops 405995520 | bytes 3024384 | tf_op jit(solution)/shard_map/dot_general | solution.py:122
  15.7 2.6 %fusion.40 = (f32[256]{0:T(256)S(1)}, f32[384,256]{0,1:T(8,128)S(1)}) fusion(f32[384,256]{0,1:T(8,128)S(1)} %copy.42, f32[256]{0:T(256)S(1)} %copy-done.8, bf16[32,1024]{1,0:T(8,128)(2,1)} %param.24, s32[]{:T(128)S(6)} %select_n.19, bf16[2048,32]{0,1:T(8,128)(2,1)} %param.23, bf16[384,2048]{1,0:T(8,128)(2,1)} %param.17, f32[2048]{0:T(1024)} %param.18, ...), kind=kOutput, calls=%fused_computation.68 | convolution fusion | flops 60960512 | bytes 2518532 | tf_op jit(solution)/shard_map/dot_general | solution.py:133
  19.5 4.0 %fusion.23 = f32[384,512]{1,0:T(8,128)} fusion(bf16[2048,512]{1,0:T(8,128)(2,1)} %param.21, bf16[384,2048]{1,0:T(8,128)(2,1)} %param.17, f32[2048]{0:T(1024)} %param.18, f32[384]{0:T(512)S(1)} %add_rsqrt_fusion.2), kind=kOutput, calls=%fused_computation.40 | convolution fusion | flops 808845312 | bytes 4466176 | tf_op jit(solution)/shard_map/dot_general | solution.py:122
  23.5 1.6 %reshape.75 = f32[6,64,2,256]{3,2,1,0:T(2,128)S(1)} reshape(f32[384,512]{1,0:T(8,128)} %fusion.23) | data formatting | bytes 1572864 | tf_op jit(solution)/shard_map/reshape;reshape | solution.py:42
  25.1 23.1 %while.26 = (s32[]{:T(128)}, f32[2,128,256]{2,1,0:T(8,128)S(1)}, f32[6,64,2,256]{3,1,0,2:T(8,128)}, f32[6,64,2,128]{3,2,1,0:T(2,128)}, f32[6,64,2,128]{3,2,1,0:T...) while((s32[]{:T(128)}, f32[2,128,256]{2,1,0:T(8,128)S(1)}, ...), condition=%wide.region_3.4_spmd.clone, body=%wide.region_1.3_spmd.clone.sunk | while | flops 139833344 | bytes 2570368 | solution.py:60
  26.1 1.0 bitcast_multiply_fusion.5
  29.9 1.0 bitcast_multiply_fusion.5
  33.7 1.0 bitcast_multiply_fusion.5
  37.6 1.0 bitcast_multiply_fusion.5
  41.4 1.0 bitcast_multiply_fusion.5
  45.3 1.0 bitcast_multiply_fusion.5
  49.9 1.1 copy.47
  52.4 1.4 copy.52
  53.8 22.5 %all_gather.13 = f32[8,2,128]{2,1,0:T(2,128)S(1)} all-gather(f32[1,2,128]{2,1,0:T(2,128)S(1)} %exponential_bitcast_fusion), channel_id=1, replica_groups=mesh['sp'=8,'tp'=4] {'sp'}, dimensions={0}, use_global_device_ids=true | all-gather | bytes 9216 | tf_op jit(solution)/shard_map/all_gather | solution.py:19
  76.2 1.2 bitcast_multiply_fusion.3
  77.4 23.6 %all-gather.6.cloned.1.call-done = f32[16,128,256]{2,1,0:T(8,128)} async-done(((f32[2,128,256]{2,1,0:T(8,128)}), f32[16,128,256]{2,1,0:T(8,128)}) %all-gather.6.cloned.1.call-update) | async-done | bytes 2097168 | tf_op jit(solution)/shard_map/all_gather | solution.py:19
  101.0 1.0 multiply_reduce_fusion.1
  102.2 1.1 copy.53
  103.3 4.1 %multiply_convert_fusion.1 = bf16[384,512]{1,0:T(8,128)(2,1)} fusion(f32[384,512]{1,0:T(8,128)} %copy.53, bf16[2048,512]{1,0:T(8,128)(2,1)} %param.22, bf16[384,2048]{1,0:T(8,128)(2,1)} %param.17, f32[2048]{0:T(1024)S(1)} %copy-done.7, f32[384]{0:T(512)S(1)} %add_rsqrt_fusion.2), kind=kOutput, calls=%fused_computation.51 | convolution fusion | flops 810024960 | bytes 4859392 | tf_op jit(solution)/shard_map/dot_general | solution.py:122
  107.5 26.1 %all-gather.4.cloned.1.call-done = bf16[384,2048]{1,0:T(8,128)(2,1)} async-done(((bf16[384,512]{1,0:T(8,128)(2,1)}), bf16[384,2048]{1,0:T(8,128)(2,1)}) %all-gather.4.cloned.1.call-update) | async-done | bytes 1572880 | tf_op jit(solution)/shard_map/all_gather | solution.py:149
  133.6 2.5 %multiply_reduce_fusion = (f32[384]{0:T(512)S(1)}, f32[384,512]{1,0:T(8,128)S(1)}) fusion(bf16[384,2048]{1,0:T(8,128)(2,1)} %all-gather.4.cloned.1.call-done, bf16[2048,512]{1,0:T(8,128)(2,1)S(1)} %copy-done), kind=kOutput, calls=%fused_computation.50 | convolution fusion | flops 805699200 | bytes 4457984 | tf_op jit(solution)/shard_map/dot_general | solution.py:148
  136.0 5.9 %psum.7 = f32[384]{0:T(512)S(1)} all-reduce(f32[384]{0:T(512)S(1)} %get-tuple-element.173), channel_id=1, replica_groups=mesh['sp'=8,'tp'=4] {'tp'}, use_global_device_ids=true, to_apply=%region_11.12 | all-reduce | flops 384 | bytes 3072 | tf_op jit(solution)/shard_map/psum | solution.py:153
  (99 shorter events, 24.3 us)
Async XLA Ops:
  6.5 127.0 %copy-start = (bf16[2048,512]{1,0:T(8,128)(2,1)S(1)}, bf16[2048,512]{1,0:T(8,128)(2,1)}, u32[]{:S(2)}) copy-start(bf16[2048,512]{1,0:T(8,128)(2,1)} %param.28) | copy-start | bytes 6291460
  6.5 94.4 %all-gather.6.cloned.1.call-start = ((), (), s32[]{:S(2)}) async-start(), calls=%async_computation.1 | async-start | bytes 2359296 | tf_op jit(solution)/shard_map/all_gather | solution.py:19
  8.5 3.7 %copy-start.6 = (f32[2048]{0:T(1024)S(1)}, f32[2048]{0:T(1024)}, u32[]{:S(2)}) copy-start(f32[2048]{0:T(1024)} %param.18) | copy-start | bytes 24580
  12.2 3.3 %copy-start.3 = (f32[384,256]{1,0:T(8,128)S(1)}, f32[384,256]{1,0:T(8,128)}, u32[]{:S(2)}) copy-start(f32[384,256]{1,0:T(8,128)} %param.26) | copy-start | bytes 1179652
  12.2 3.5 %copy-start.8 = (f32[256]{0:T(256)S(1)}, f32[256]{0:T(256)}, u32[]{:S(2)}) copy-start(f32[256]{0:T(256)} %param.25) | copy-start | bytes 3076
  18.3 1.1 copy-start.2
  25.1 23.9 %copy-start.5 = (f32[512]{0:T(512)S(1)}, f32[512]{0:T(512)}, u32[]{:S(2)}) copy-start(f32[512]{0:T(512)} %param.27) | copy-start | bytes 6148
  48.2 0.7 copy-start.1
  48.9 84.7 %all-gather.4.cloned.1.call-start = ((), (), s32[]{:S(2)}) async-start(), calls=%async_computation | async-start | bytes 1966080 | tf_op jit(solution)/shard_map/all_gather | solution.py:149
  102.0 1.3 copy-start.7
  107.5 34.4 %copy-start.4 = (f32[512]{0:T(512)S(1)}, f32[512]{0:T(512)}, u32[]{:S(2)}) copy-start(f32[512]{0:T(512)} %param.29) | copy-start | bytes 6148
Sparse Core Ops, SparseCore 0:
  49.0 51.8 all-gather.5
  107.6 25.9 all-gather.3
where the time goes:
time: 151 us; the launch traced here: 150 us
  waiting for transfers between devices  49.7 us (33%)
  matrix products  30.3 us (20%)
  blocking collectives  28.3 us (19%)
  other arithmetic  16.1 us (11%)
  between operations  13.6 us (9%)
  local copies, waits for them, and re-layouts  11.3 us (7%)
    all_gather x1, waiting for transfers between devices, local(): lax.all_gather(gated, 'tp', axis=1, tiled=True)  26.1 us
    all_gather x1, waiting for transfers between devices, entering(): gathered = jax.tree.map(lambda a: lax.all_gather(a, axis), part)  23.6 us
    all_gather x1, blocking collectives, entering(): gathered = jax.tree.map(lambda a: lax.all_gather(a, axis), part)  22.5 us
    dot_general x4, matrix products, project(): jnp.dot(normed, weight, preferred_element_type=jnp.float32)  13.1 us
    mul x6, other arithmetic, block_step(): key_inner = key_block * jnp.exp(-cumulative)  5.94 us
    psum x1, blocking collectives, local(): squares = lax.psum(jnp.sum(mixed * mixed, axis=1), 'tp')  5.88 us
    dot_general x6, matrix products, block_step(): output = jnp.einsum('hcs,she->che', scores, value_block, precision=highest)  5.55 us
    another operation x6, other arithmetic, block_step(): cumulative = jnp.cumsum(decay_block, axis=0)  5.48 us
  transfers between devices with their start and end apart: 2, of which 2 were waited for; matrix products, arithmetic and copies ran while one was open for 4% of the time, Pallas kernels for 0%

commit v1 on v0

v1 whole, which is shorter than its diff:
```python
import functools

import jax
import jax.numpy as jnp
from jax import lax
from jax.experimental import pallas as pl
from jax.experimental.pallas import tpu as pltpu
from jax.sharding import PartitionSpec as P

QUERY_FEATURES = 128
DV = 256
BLOCK = 128
PAD = 16

norm_eps = 1e-06
decay_temper = 16.0
highest = lax.Precision.HIGHEST
f32 = jnp.float32
bf16 = jnp.bfloat16
VMEM = pltpu.VMEM
ANY = pl.ANY


def mm(a, b):
    return jnp.dot(a, b, preferred_element_type=f32)


def mm_t(a, b):
    return lax.dot_general(a, b, (((1,), (1,)), ((), ())), preferred_element_type=f32)


def mm_l(a, b):
    return lax.dot_general(a, b, (((0,), (0,)), ((), ())), preferred_element_type=f32)


def kernel_a(
    heads,
    tok_hbm,
    gain_ref,
    wk_hbm,
    wv_hbm,
    down_ref,
    up_hbm,
    off_ref,
    extra_hbm,
    normed_hbm,
    k_hbm,
    v_hbm,
    c_hbm,
    *rest,
):
    msgs = rest[:heads]
    tok, wk, wv, up, extra, normed, kb, vb, cb, sems = rest[heads:]
    rows = tok.shape[0]
    width = heads * QUERY_FEATURES
    place = lax.axis_index("tp")
    columns = pl.ds(pl.multiple_of(place * width, QUERY_FEATURES), width)
    loads = [
        pltpu.make_async_copy(tok_hbm, tok, sems.at[0]),
        pltpu.make_async_copy(up_hbm.at[:, columns], up, sems.at[1]),
        pltpu.make_async_copy(extra_hbm, extra, sems.at[2]),
        pltpu.make_async_copy(wk_hbm, wk, sems.at[3]),
        pltpu.make_async_copy(wv_hbm, wv, sems.at[4]),
    ]
    for load in loads:
        load.start()
    loads[0].wait()
    gain = gain_ref[...]
    for r in range(0, rows, BLOCK):
        wide = tok[r : r + BLOCK, :].astype(f32)
        scale = lax.rsqrt(jnp.mean(wide * wide, axis=1, keepdims=True) + norm_eps)
        normed[r : r + BLOCK, :] = (wide * scale * gain).astype(bf16)
    stores = [pltpu.make_async_copy(normed, normed_hbm, sems.at[5])]
    stores[0].start()
    low = mm(normed[...], down_ref[...]).astype(bf16)
    loads[1].wait()
    loads[2].wait()
    logits = mm(low, up[...]) + off_ref[...]
    soft = jnp.minimum(logits, 0.0) - jnp.log1p(jnp.exp(-jnp.abs(logits)))
    decay = soft / decay_temper + extra[...]
    i0 = lax.broadcasted_iota(jnp.int32, (BLOCK, BLOCK), 0)
    i1 = lax.broadcasted_iota(jnp.int32, (BLOCK, BLOCK), 1)
    lower = jnp.where(i0 >= i1, 1.0, 0.0).astype(f32)
    total = jnp.zeros((1, width), f32)
    for r in range(0, rows, BLOCK):
        block = (
            lax.dot_general(
                lower,
                decay[r : r + BLOCK, :],
                (((1,), (0,)), ((), ())),
                precision=highest,
                preferred_element_type=f32,
            )
            + total
        )
        cb[r : r + BLOCK, :] = block
        total = block[BLOCK - 1 : BLOCK, :]
    stores.append(pltpu.make_async_copy(cb, c_hbm, sems.at[6]))
    stores[1].start()
    fade = jnp.exp(total - cb[...])
    closing = jnp.exp(total)
    high = closing.astype(bf16)
    rest_of = (closing - high.astype(f32)).astype(bf16)
    loads[3].wait()
    kb[...] = mm(normed[...], wk[...]).astype(bf16)
    stores.append(pltpu.make_async_copy(kb, k_hbm, sems.at[7]))
    stores[2].start()
    faded = (kb[...].astype(f32) * fade).astype(bf16)
    loads[4].wait()
    row = lax.broadcasted_iota(jnp.int32, (PAD, QUERY_FEATURES), 0)
    for h in range(heads):
        cv = slice(h * DV, (h + 1) * DV)
        ck = slice(h * QUERY_FEATURES, (h + 1) * QUERY_FEATURES)
        vb[:, cv] = mm(normed[...], wv[:, cv]).astype(bf16)
        msgs[h][:DV, :] = mm_l(vb[:, cv], faded[:, ck]).astype(bf16)
        tail = jnp.where(
            row == 0,
            high[:, ck].astype(f32),
            jnp.where(row == 1, rest_of[:, ck].astype(f32), 0.0),
        )
        msgs[h][DV:, :] = tail.astype(bf16)
    stores.append(pltpu.make_async_copy(vb, v_hbm, sems.at[8]))
    stores[3].start()
    for store in stores:
        store.wait()


def local_states(
    tokens, in_gain, key_weight, value_weight, decay_down, decay_up, decay_offset, decay_extra
):
    rows, model = tokens.shape
    width = key_weight.shape[1]
    values = value_weight.shape[1]
    heads = width // QUERY_FEATURES
    out_shape = [
        jax.ShapeDtypeStruct((rows, model), bf16),
        jax.ShapeDtypeStruct((rows, width), bf16),
        jax.ShapeDtypeStruct((rows, values), bf16),
        jax.ShapeDtypeStruct((rows, width), f32),
    ] + [jax.ShapeDtypeStruct((DV + PAD, QUERY_FEATURES), bf16)] * heads
    vm = pl.BlockSpec(memory_space=VMEM)
    hb = pl.BlockSpec(memory_space=ANY)
    return pl.pallas_call(
        functools.partial(kernel_a, heads),
        out_shape=out_shape,
        in_specs=[hb, vm, hb, hb, vm, hb, vm, hb],
        out_specs=[hb] * 4 + [vm] * heads,
        scratch_shapes=[
            VMEM((rows, model), bf16),
            VMEM((model, width), bf16),
            VMEM((model, values), bf16),
            VMEM((decay_up.shape[0], width), bf16),
            VMEM((rows, width), f32),
            VMEM((rows, model), bf16),
            VMEM((rows, width), bf16),
            VMEM((rows, values), bf16),
            VMEM((rows, width), f32),
            pltpu.SemaphoreType.DMA((9,)),
        ],
        compiler_params=pltpu.CompilerParams(vmem_limit_bytes=24 << 20),
        cost_estimate=pl.CostEstimate(
            flops=2 * rows * model * (width + values), bytes_accessed=8 << 20, transcendentals=0
        ),
        name="states",
    )(
        tokens,
        in_gain[None, :],
        key_weight,
        value_weight,
        decay_down,
        decay_up,
        decay_offset[None, :],
        decay_extra,
    )


def kernel_b(heads, normed, wq, wg, k, v, c, gain, *outs):
    locals_, queries, gates = outs[:heads], outs[heads : 2 * heads], outs[2 * heads :]
    rows = normed.shape[0]
    i0 = lax.broadcasted_iota(jnp.int32, (BLOCK, BLOCK), 0)
    i1 = lax.broadcasted_iota(jnp.int32, (BLOCK, BLOCK), 1)
    causal = i0 >= i1
    q_all = mm(normed[...], wq[...]).astype(bf16).astype(f32)
    for h in range(heads):
        ck = slice(h * QUERY_FEATURES, (h + 1) * QUERY_FEATURES)
        cv = slice(h * DV, (h + 1) * DV)
        q_head = q_all[:, ck]
        state = None
        start = None
        for r in range(0, rows, BLOCK):
            rs = slice(r, r + BLOCK)
            q = q_head[rs, :]
            kk = k[rs, ck].astype(f32)
            vv = v[rs, cv]
            cc = c[rs, ck]
            middle = c[r + BLOCK // 2 - 1 : r + BLOCK // 2, ck]
            end = c[r + BLOCK - 1 : r + BLOCK, ck]
            queries[h][rs, :] = (q * jnp.exp(cc)).astype(bf16)
            q_mid = (q * jnp.exp(cc - middle)).astype(bf16)
            k_mid = (kk * jnp.exp(middle - cc)).astype(bf16)
            scores = jnp.where(causal, mm_t(q_mid, k_mid), 0.0).astype(bf16)
            out = mm(scores, vv)
            if state is not None:
                out = out + mm_t((q * jnp.exp(cc - start)).astype(bf16), state.astype(bf16))
            locals_[h][rs, :] = out
            if r + BLOCK < rows:
                k_end = (kk * jnp.exp(end - cc)).astype(bf16)
                added = mm_l(vv, k_end)
                state = added if state is None else state * jnp.exp(end - start) + added
                start = end
        gate = mm(normed[...], wg[:, cv]).astype(bf16).astype(f32)
        gates[h][...] = gain[:, cv] * (gate * jax.nn.sigmoid(gate))


def local_attention(normed, query_weight, gate_weight, k, v, c, head_gain):
    rows, model = normed.shape
    width = query_weight.shape[1]
    values = gate_weight.shape[1]
    heads = width // QUERY_FEATURES
    vm = pl.BlockSpec(memory_space=VMEM)
    return pl.pallas_call(
        functools.partial(kernel_b, heads),
        out_shape=[jax.ShapeDtypeStruct((rows, DV), f32)] * heads
        + [jax.ShapeDtypeStruct((rows, QUERY_FEATURES), bf16)] * heads
        + [jax.ShapeDtypeStruct((rows, DV), f32)] * heads,
        in_specs=[vm] * 7,
        out_specs=[vm] * (3 * heads),
        compiler_params=pltpu.CompilerParams(vmem_limit_bytes=24 << 20),
        cost_estimate=pl.CostEstimate(
            flops=2 * rows * model * (width + values), bytes_accessed=8 << 20, transcendentals=0
        ),
        name="attention",
    )(normed, query_weight, gate_weight, k, v, c, head_gain[None, :])


def kernel_c(loc, q, state, gate, out):
    att = loc[...] + mm_t(q[...], state[...])
    scale = lax.rsqrt(jnp.mean(att * att, axis=1, keepdims=True) + norm_eps)
    out[...] = (att * scale * gate[...]).astype(bf16)


def finish_head(loc, q, state, gate):
    vm = pl.BlockSpec(memory_space=VMEM)
    return pl.pallas_call(
        kernel_c,
        out_shape=jax.ShapeDtypeStruct(loc.shape, bf16),
        in_specs=[vm] * 4,
        out_specs=vm,
        compiler_params=pltpu.CompilerParams(vmem_limit_bytes=8 << 20),
        cost_estimate=pl.CostEstimate(
            flops=2 * loc.shape[0] * DV * QUERY_FEATURES, bytes_accessed=1 << 20, transcendentals=0
        ),
        name="finish",
    )(loc, q, state, gate)


def swap(value, axis, count, bit):
    return lax.ppermute(value, axis, [(i, i ^ bit) for i in range(count)])


def turn(value, axis, count, by):
    return lax.ppermute(value, axis, [(i, (i + by) % count) for i in range(count)])


def split(message):
    decay = message[DV : DV + 1].astype(f32) + message[DV + 1 : DV + 2].astype(f32)
    return message[:DV].astype(f32), decay


def join(state, decay):
    high = decay.astype(bf16)
    low = (decay - high.astype(f32)).astype(bf16)
    pad = jnp.zeros((PAD - 2, decay.shape[1]), bf16)
    return jnp.concatenate([state.astype(bf16), high, low, pad], axis=0)


def entering(messages, count):
    place = lax.axis_index("sp")
    totals = list(messages)
    heads = len(totals)
    entered = [None] * heads
    before = [None] * heads
    bit = 1
    while bit < count:
        later = (place & bit) != 0
        received = [swap(m, "sp", count, bit) for m in totals]
        for h in range(heads):
            state, decay = split(received[h])
            own_state, own_decay = split(totals[h])
            if entered[h] is None:
                entered[h] = jnp.where(later, state, 0.0)
                before[h] = jnp.where(later, decay, 1.0)
            else:
                entered[h] = jnp.where(later, entered[h] + before[h] * state, entered[h])
                before[h] = jnp.where(later, before[h] * decay, before[h])
            if 2 * bit < count:
                totals[h] = join(
                    jnp.where(later, own_decay * state + own_state, decay * own_state + state),
                    own_decay * decay,
                )
        bit *= 2
    return [e.astype(bf16) for e in entered]


def local(
    sp,
    tp,
    tokens,
    in_gain,
    query_weight,
    key_weight,
    value_weight,
    gate_weight,
    decay_down,
    decay_up,
    decay_offset,
    decay_extra,
    head_gain,
    out_weight,
    out_gain,
):
    heads = query_weight.shape[1] // QUERY_FEATURES
    values = value_weight.shape[1]
    normed, k, v, c, *messages = local_states(
        tokens, in_gain, key_weight, value_weight, decay_down, decay_up, decay_offset, decay_extra
    )
    outs = local_attention(normed, query_weight, gate_weight, k, v, c, head_gain)
    locals_, queries, gates = outs[:heads], outs[heads : 2 * heads], outs[2 * heads :]
    states = entering(messages, sp)
    place = lax.axis_index("tp")
    mixed = 0.0
    for h in range(heads):
        gated = finish_head(locals_[h], queries[h], states[h], gates[h])

        def add(mixed, piece, owner):
            start = owner * values + h * DV
            rows_of = lax.dynamic_slice_in_dim(out_weight, start, DV, 0)
            return mixed + mm(piece, rows_of)

        mixed = add(mixed, gated, place)
        mixed = add(mixed, swap(gated, "tp", tp, 1), place ^ 1)
        for by in range(2, tp, 2):
            piece = turn(gated, "tp", tp, by)
            owner = (place - by) % tp
            mixed = add(mixed, piece, owner)
            mixed = add(mixed, swap(piece, "tp", tp, 1), owner ^ 1)
    squares = jnp.sum(mixed * mixed, axis=1, keepdims=True)
    part = squares.reshape(-1, QUERY_FEATURES)
    whole = part
    for by in range(1, tp):
        whole = whole + turn(part, "tp", tp, by)
    squares = whole.reshape(-1, 1)
    out_width = tp * out_weight.shape[1]
    result = mixed * lax.rsqrt(squares / out_width + norm_eps) * out_gain
    return result.astype(bf16)


def solution(mesh):
    placed = (
        P("sp", None),
        P(),
        P(None, "tp"),
        P(None, "tp"),
        P(None, "tp"),
        P(None, "tp"),
        P(),
        P(),
        P("tp"),
        P("sp", "tp"),
        P("tp"),
        P(None, "tp"),
        P("tp"),
    )
    return jax.shard_map(
        functools.partial(local, mesh.shape["sp"], mesh.shape["tp"]),
        mesh=mesh,
        in_specs=placed,
        out_specs=P("sp", "tp"),
        check_vma=False,
    )
```

time: 151 us -> 63.8 us (0.42)
  waiting for transfers between devices: 49.7 us -> 17.7 us
  blocking collectives: 28.3 us -> 0 us
  matrix products: 30.3 us -> 2.16 us
  starting transfers between devices: 0.04 us -> 16.1 us
  other arithmetic: 16.1 us -> 1.54 us
  between operations: 13.6 us -> 0.25 us
  Pallas kernels: 0 us -> 9.67 us
  local copies, waits for them, and re-layouts: 11.3 us -> 15.8 us
    all_gather x2 -> x0, waiting for transfers between devices: 49.6 us -> none  [the longest x1 26.1 us: local(): lax.all_gather(gated, 'tp', axis=1, tiled=True)]
    dot_general x31 -> x8, matrix products: 30.3 us -> 2.16 us  [mm(): return jnp.dot(a, b, preferred_element_type=f32)]
    all_gather x1 -> x0, blocking collectives: 22.5 us -> none  [entering(): gathered = jax.tree.map(lambda a: lax.all_gather(a, axis), part)]
    ppermute x0 -> x15, waiting for transfers between devices: none -> 17.7 us  [the longest x10 11.9 us: swap(): return lax.ppermute(value, axis, [(i, i ^ bit) for i in range(count)])]
    ppermute x0 -> x15, starting transfers between devices: none -> 16.1 us  [the longest x10 11.1 us: swap(): return lax.ppermute(value, axis, [(i, i ^ bit) for i in range(count)])]
    unnamed x19 -> x33, local copies, waits for them, and re-layouts: 0.9 us -> 15.8 us
    pallas_call x0 -> x4, Pallas kernels: none -> 9.67 us  [the longest x1 6.89 us: local_states(): pl.pallas_call(functools.partial(kernel_a, heads), out_shape=out_shape, i...]
    mul x8 -> x6, other arithmetic: 7.23 us -> 0.05 us  [the longest x4 0.03 us: entering(): entered[h] = jnp.where(later, entered[h] + before[h] * state, entered[h])]
  transfers between devices with their start and end apart: 2 -> 15, of which waited for: 2 -> 8; matrix products, arithmetic and copies ran while one was open for 4% -> 4% of each run, Pallas kernels for 0% -> 4%
where the time goes in v1:
time: 63.8 us; the launch traced here: 63.3 us
  waiting for transfers between devices  17.7 us (28%)
  starting transfers between devices  16.1 us (25%)
  local copies, waits for them, and re-layouts  15.8 us (25%)
  Pallas kernels  9.67 us (15%)
  matrix products  2.16 us (3%)
  other arithmetic  1.54 us (2%)
    unnamed x33, local copies, waits for them, and re-layouts  15.8 us
    ppermute x10, waiting for transfers between devices, swap(): return lax.ppermute(value, axis, [(i, i ^ bit) for i in range(count)])  11.9 us
    ppermute x10, starting transfers between devices, swap(): return lax.ppermute(value, axis, [(i, i ^ bit) for i in range(count)])  11.1 us
    pallas_call x1, Pallas kernels, local_states(): pl.pallas_call(functools.partial(kernel_a, heads), out_shape=out_shape, i...  6.89 us
    ppermute x5, waiting for transfers between devices, turn(): lax.ppermute(value, axis, [(i, (i + by) % count) for i in range(count)])  5.86 us
    ppermute x5, starting transfers between devices, turn(): lax.ppermute(value, axis, [(i, (i + by) % count) for i in range(count)])  4.94 us
    pallas_call x1, Pallas kernels, local_attention(): pl.pallas_call(functools.partial(kernel_b, heads), out_shape=[jax.ShapeDt...  2.17 us
    dot_general x8, matrix products, mm(): return jnp.dot(a, b, preferred_element_type=f32)  2.16 us
  transfers between devices with their start and end apart: 15, of which 8 were waited for; matrix products, arithmetic and copies ran while one was open for 4% of the time, Pallas kernels for 4%

profile of v1, /device:TPU:0, one launch (start us, length us, event | category | flops | bytes accessed | tf_op | source)
XLA Modules:
  0.0 63.3 jit_solution(17872381764425193084)
XLA Ops:
  0.0 1.3 %copy.14.down_ref = bf16[2048,32]{1,0:T(8,128)(2,1)S(1)} copy(bf16[2048,32]{0,1:T(8,128)(2,1)} %param.19) | data formatting | bytes 262144 | tf_op args[6]
  1.3 1.6 %copy-done.1 = bf16[2048,512]{1,0:T(8,128)(2,1)S(1)} copy-done((bf16[2048,512]{1,0:T(8,128)(2,1)S(1)}, bf16[2048,512]{1,0:T(8,128)(2,1)}, u32[]{:S(2)}) %copy-start.1) | copy-done | bytes 2097176
  2.9 1.4 %copy-done.3 = bf16[384,2048]{1,0:T(8,128)(2,1)S(1)} copy-done((bf16[384,2048]{1,0:T(8,128)(2,1)S(1)}, bf16[384,2048]{1,0:T(8,128)(2,1)}, u32[]{:S(2)}) %copy-start.3) | copy-done | bytes 1572888
  4.3 1.2 %copy-done.6 = bf16[2048,256]{1,0:T(8,128)(2,1)S(1)} copy-done((bf16[2048,256]{1,0:T(8,128)(2,1)S(1)}, bf16[2048,256]{1,0:T(8,128)(2,1)}, u32[]{:S(2)}) %copy-start.6) | copy-done | bytes 1048600
  5.6 1.0 %copy-done.8 = f32[384,256]{1,0:T(8,128)S(1)} copy-done((f32[384,256]{1,0:T(8,128)S(1)}, f32[384,256]{1,0:T(8,128)}, u32[]{:S(2)}) %copy-start.8) | copy-done | bytes 393240
  8.8 6.9 %states.1 = (bf16[384,2048]{1,0:T(8,128)(2,1)S(1)}, bf16[384,256]{1,0:T(8,128)(2,1)S(1)}, bf16[384,512]{1,0:T(8,128)(2,1)S(1)}, f32[384,256]{1,0:T(8,128)S(1)}, ...) custom-call(bf16[384,2048]{1,0:T(8,128)(2,1)S(1)} %copy-done.3, f32[1,2048]{1,0:T(1,128)S(1)} %bitcast.35, ...), custom_call_target="tpu_custom_call" | custom-call | flops 1207959552 | bytes 8388608 | tf_op jit(solution)/shard_map/states/pallas_call | solution.py:143
  15.7 1.2 %copy-done.4 = bf16[384,2048]{1,0:T(8,128)(2,1)} copy-done((bf16[384,2048]{1,0:T(8,128)(2,1)}, bf16[384,2048]{1,0:T(8,128)(2,1)S(1)}, u32[]{:S(2)}) %copy-start.4) | copy-done | bytes 1572888
  17.5 3.0 %collective-permute-start = (bf16[272,128]{1,0:T(8,128)(2,1)S(1)}, bf16[272,128]{1,0:T(8,128)(2,1)S(1)}, u32[]{:S(2)}, u32[]{:S(2)}) collective-permute-start(bf16[272,128]{1,0:T(8,128)(2,1)S(1)} %get-tuple-element.23), channel_id=1, source_target_pairs={{0,4},{4,0},{8,12},{12,8},{16,20},{20,16},{24,28},{28,24},{1,5},{5... | collective-permute-start | bytes 208904 | tf_op jit(solution)/shard_map/ppermute | solution.py:258
  20.6 2.3 %collective-permute-done = bf16[272,128]{1,0:T(8,128)(2,1)S(1)} collective-permute-done((bf16[272,128]{1,0:T(8,128)(2,1)S(1)}, bf16[272,128]{1,0:T(8,128)(2,1)S(1)}, u32[]{:S(2)}, u32[]{:S(2)}) %collective-permute-start) | collective-permute-done | bytes 69664 | tf_op jit(solution)/shard_map/ppermute | solution.py:258
  23.1 2.6 %collective-permute-start.1 = (bf16[272,128]{1,0:T(8,128)(2,1)S(1)}, bf16[272,128]{1,0:T(8,128)(2,1)S(1)}, u32[]{:S(2)}, u32[]{:S(2)}) collective-permute-start(bf16[272,128]{1,0:T(8,128)(2,1)S(1)} %maximum_maximum_fusion), channel_id=1, source_target_pairs={{0,8},{4,12},{8,0},{12,4},{16,24},{20,28},{24,16},{28,20},{1,9},{5... | collective-permute-start | bytes 208904 | tf_op jit(solution)/shard_map/ppermute | solution.py:258
  25.9 2.2 %collective-permute-done.1 = bf16[272,128]{1,0:T(8,128)(2,1)S(1)} collective-permute-done((bf16[272,128]{1,0:T(8,128)(2,1)S(1)}, bf16[272,128]{1,0:T(8,128)(2,1)S(1)}, u32[]{:S(2)}, u32[]{:S(2)}) %collective-permute-start.1) | collective-permute-done | bytes 69664 | tf_op jit(solution)/shard_map/ppermute | solution.py:258
  28.3 3.5 %collective-permute-start.2 = (bf16[272,128]{1,0:T(8,128)(2,1)S(1)}, bf16[272,128]{1,0:T(8,128)(2,1)S(1)}, u32[]{:S(2)}, u32[]{:S(2)}) collective-permute-start(bf16[272,128]{1,0:T(8,128)(2,1)S(1)} %get-tuple-element.43), channel_id=1, source_target_pairs={{0,16},{4,20},{8,24},{12,28},{16,0},{20,4},{24,8},{28,12},{1,17},{... | collective-permute-start | bytes 208904 | tf_op jit(solution)/shard_map/ppermute | solution.py:258
  31.7 1.6 %copy-done.2 = bf16[2048,512]{1,0:T(8,128)(2,1)S(1)} copy-done((bf16[2048,512]{1,0:T(8,128)(2,1)S(1)}, bf16[2048,512]{1,0:T(8,128)(2,1)}, u32[]{:S(2)}) %copy-start.2) | copy-done | bytes 2097176
  33.3 1.4 %copy-done.5 = bf16[384,2048]{1,0:T(8,128)(2,1)S(1)} copy-done((bf16[384,2048]{1,0:T(8,128)(2,1)S(1)}, bf16[384,2048]{1,0:T(8,128)(2,1)}, u32[]{:S(2)}) %copy-start.5) | copy-done | bytes 1572888
  34.7 1.2 %copy-done.7 = bf16[2048,256]{1,0:T(8,128)(2,1)S(1)} copy-done((bf16[2048,256]{1,0:T(8,128)(2,1)S(1)}, bf16[2048,256]{1,0:T(8,128)(2,1)}, u32[]{:S(2)}) %copy-start.7) | copy-done | bytes 1048600
  36.9 2.2 %attention.1 = (f32[384,256]{1,0:T(8,128)S(1)}, f32[384,256]{1,0:T(8,128)S(1)}, bf16[384,128]{1,0:T(8,128)(2,1)S(1)}, bf16[384,128]{1,0:T(8,128)(2,1)S(1)}, f32[...) custom-call(bf16[384,2048]{1,0:T(8,128)(2,1)S(1)} %copy-done.5, bf16[2048,256]{1,0:T(8,128)(2,1)S(1)} %copy-done.7, ...), custom_call_target="tpu_custom_call" | custom-call | flops 1207959552 | bytes 8388608 | tf_op jit(solution)/shard_map/attention/pallas_call | solution.py:221
  39.1 1.3 %collective-permute-start.7 = (bf16[272,128]{1,0:T(8,128)(2,1)S(1)}, bf16[272,128]{1,0:T(8,128)(2,1)S(1)}, u32[]{:S(2)}, u32[]{:S(2)}) collective-permute-start(bf16[272,128]{1,0:T(8,128)(2,1)S(1)} %get-tuple-element.44), channel_id=1, source_target_pairs={{0,8},{4,12},{8,0},{12,4},{16,24},{20,28},{24,16},{28,20},{1,9},{5... | collective-permute-start | bytes 208904 | tf_op jit(solution)/shard_map/ppermute | solution.py:258
  40.8 1.6 %collective-permute-start.4 = (bf16[384,256]{1,0:T(8,128)(2,1)S(1)}, bf16[384,256]{1,0:T(8,128)(2,1)S(1)}, u32[]{:S(2)}, u32[]{:S(2)}) collective-permute-start(bf16[384,256]{1,0:T(8,128)(2,1)S(1)} %finish.2), channel_id=1, source_target_pairs={{0,2},{1,3},{2,0},{3,1},{4,6},{5,7},{6,4},{7,5},{8,10},{9,11},{10,... | collective-permute-start | bytes 589832 | tf_op jit(solution)/shard_map/ppermute | solution.py:262
  42.3 1.1 %collective-permute-done.7 = bf16[272,128]{1,0:T(8,128)(2,1)S(1)} collective-permute-done((bf16[272,128]{1,0:T(8,128)(2,1)S(1)}, bf16[272,128]{1,0:T(8,128)(2,1)S(1)}, u32[]{:S(2)}, u32[]{:S(2)}) %collective-permute-start.7) | collective-permute-done | bytes 69664 | tf_op jit(solution)/shard_map/ppermute | solution.py:258
  44.0 5.7 %collective-permute-done.8 = bf16[272,128]{1,0:T(8,128)(2,1)S(1)} collective-permute-done((bf16[272,128]{1,0:T(8,128)(2,1)S(1)}, bf16[272,128]{1,0:T(8,128)(2,1)S(1)}, u32[]{:S(2)}, u32[]{:S(2)}) %collective-permute-start.8) | collective-permute-done | bytes 69664 | tf_op jit(solution)/shard_map/ppermute | solution.py:258
  50.0 1.6 %collective-permute-start.10 = (bf16[384,256]{1,0:T(8,128)(2,1)S(1)}, bf16[384,256]{1,0:T(8,128)(2,1)S(1)}, u32[]{:S(2)}, u32[]{:S(2)}) collective-permute-start(bf16[384,256]{1,0:T(8,128)(2,1)S(1)} %finish.3), channel_id=1, source_target_pairs={{0,2},{1,3},{2,0},{3,1},{4,6},{5,7},{6,4},{7,5},{8,10},{9,11},{10,... | collective-permute-start | bytes 589832 | tf_op jit(solution)/shard_map/ppermute | solution.py:262
  52.9 2.8 %collective-permute-done.10 = bf16[384,256]{1,0:T(8,128)(2,1)S(1)} collective-permute-done((bf16[384,256]{1,0:T(8,128)(2,1)S(1)}, bf16[384,256]{1,0:T(8,128)(2,1)S(1)}, u32[]{:S(2)}, u32[]{:S(2)}) %collective-permute-start.10) | collective-permute-done | bytes 196640 | tf_op jit(solution)/shard_map/ppermute | solution.py:262
  57.5 1.3 %collective-permute-start.14 = (f32[3,128]{1,0:T(4,128)S(1)}, f32[3,128]{1,0:T(4,128)S(1)}, u32[]{:S(2)}, u32[]{:S(2)}) collective-permute-start(f32[3,128]{1,0:T(4,128)S(1)} %bitcast.40), channel_id=1, source_target_pairs={{0,3},{1,0},{2,1},{3,2},{4,7},{5,4},{6,5},{7,6},{8,11},{9,8},{10,9... | collective-permute-start | bytes 4616 | tf_op jit(solution)/shard_map/ppermute | solution.py:262
  60.1 2.3 %collective-permute-done.13 = f32[3,128]{1,0:T(4,128)S(1)} collective-permute-done((f32[3,128]{1,0:T(4,128)S(1)}, f32[3,128]{1,0:T(4,128)S(1)}, u32[]{:S(2)}, u32[]{:S(2)}) %collective-permute-start.13) | collective-permute-done | bytes 1568 | tf_op jit(solution)/shard_map/ppermute | solution.py:262
  (74 shorter events, 10.9 us)
Async XLA Ops:
  0.0 43.7 %copy-start = (bf16[2048,512]{1,0:T(8,128)(2,1)S(1)}, bf16[2048,512]{1,0:T(8,128)(2,1)}, u32[]{:S(2)}) copy-start(bf16[2048,512]{1,0:T(8,128)(2,1)} %param.24) | copy-start | bytes 6291460
  1.3 1.6 %copy-start.1 = (bf16[2048,512]{1,0:T(8,128)(2,1)S(1)}, bf16[2048,512]{1,0:T(8,128)(2,1)}, u32[]{:S(2)}) copy-start(bf16[2048,512]{1,0:T(8,128)(2,1)} %wv_hbm.1) | copy-start | bytes 6291460
  2.9 1.4 %copy-start.3 = (bf16[384,2048]{1,0:T(8,128)(2,1)S(1)}, bf16[384,2048]{1,0:T(8,128)(2,1)}, u32[]{:S(2)}) copy-start(bf16[384,2048]{1,0:T(8,128)(2,1)} %tok_hbm.1) | copy-start | bytes 4718596
  4.3 1.2 %copy-start.6 = (bf16[2048,256]{1,0:T(8,128)(2,1)S(1)}, bf16[2048,256]{1,0:T(8,128)(2,1)}, u32[]{:S(2)}) copy-start(bf16[2048,256]{1,0:T(8,128)(2,1)} %wk_hbm.1) | copy-start | bytes 3145732
  8.8 22.9 %copy-start.13 = (f32[512]{0:T(512)S(1)}, f32[512]{0:T(512)}, u32[]{:S(2)}) copy-start(f32[512]{0:T(512)} %param.23) | copy-start | bytes 6148
  17.5 5.4 %collective-permute-start = (bf16[272,128]{1,0:T(8,128)(2,1)S(1)}, bf16[272,128]{1,0:T(8,128)(2,1)S(1)}, u32[]{:S(2)}, u32[]{:S(2)}) collective-permute-start(bf16[272,128]{1,0:T(8,128)(2,1)S(1)} %get-tuple-element.23), channel_id=1, source_target_pairs={{0,4},{4,0},{8,12},{12,8},{16,20},{20,16},{24,28},{28,24},{1,5},{5... | collective-permute-start | bytes 208904 | tf_op jit(solution)/shard_map/ppermute | solution.py:258
  20.5 5.3 %collective-permute-start.6 = (bf16[272,128]{1,0:T(8,128)(2,1)S(1)}, bf16[272,128]{1,0:T(8,128)(2,1)S(1)}, u32[]{:S(2)}, u32[]{:S(2)}) collective-permute-start(bf16[272,128]{1,0:T(8,128)(2,1)S(1)} %get-tuple-element.27), channel_id=1, source_target_pairs={{0,4},{4,0},{8,12},{12,8},{16,20},{20,16},{24,28},{28,24},{1,5},{5... | collective-permute-start | bytes 208904 | tf_op jit(solution)/shard_map/ppermute | solution.py:258
  23.1 4.9 %collective-permute-start.1 = (bf16[272,128]{1,0:T(8,128)(2,1)S(1)}, bf16[272,128]{1,0:T(8,128)(2,1)S(1)}, u32[]{:S(2)}, u32[]{:S(2)}) collective-permute-start(bf16[272,128]{1,0:T(8,128)(2,1)S(1)} %maximum_maximum_fusion), channel_id=1, source_target_pairs={{0,8},{4,12},{8,0},{12,4},{16,24},{20,28},{24,16},{28,20},{1,9},{5... | collective-permute-start | bytes 208904 | tf_op jit(solution)/shard_map/ppermute | solution.py:258
  28.3 12.1 %collective-permute-start.2 = (bf16[272,128]{1,0:T(8,128)(2,1)S(1)}, bf16[272,128]{1,0:T(8,128)(2,1)S(1)}, u32[]{:S(2)}, u32[]{:S(2)}) collective-permute-start(bf16[272,128]{1,0:T(8,128)(2,1)S(1)} %get-tuple-element.43), channel_id=1, source_target_pairs={{0,16},{4,20},{8,24},{12,28},{16,0},{20,4},{24,8},{28,12},{1,17},{... | collective-permute-start | bytes 208904 | tf_op jit(solution)/shard_map/ppermute | solution.py:258
  31.7 1.6 %copy-start.2 = (bf16[2048,512]{1,0:T(8,128)(2,1)S(1)}, bf16[2048,512]{1,0:T(8,128)(2,1)}, u32[]{:S(2)}) copy-start(bf16[2048,512]{1,0:T(8,128)(2,1)} %wg.1) | copy-start | bytes 6291460
  33.3 1.4 %copy-start.5 = (bf16[384,2048]{1,0:T(8,128)(2,1)S(1)}, bf16[384,2048]{1,0:T(8,128)(2,1)}, u32[]{:S(2)}) copy-start(bf16[384,2048]{1,0:T(8,128)(2,1)} %copy-done.4) | copy-start | bytes 4718596
  34.7 1.2 %copy-start.7 = (bf16[2048,256]{1,0:T(8,128)(2,1)S(1)}, bf16[2048,256]{1,0:T(8,128)(2,1)}, u32[]{:S(2)}) copy-start(bf16[2048,256]{1,0:T(8,128)(2,1)} %wq.1) | copy-start | bytes 3145732
  39.1 4.4 %collective-permute-start.7 = (bf16[272,128]{1,0:T(8,128)(2,1)S(1)}, bf16[272,128]{1,0:T(8,128)(2,1)S(1)}, u32[]{:S(2)}, u32[]{:S(2)}) collective-permute-start(bf16[272,128]{1,0:T(8,128)(2,1)S(1)} %get-tuple-element.44), channel_id=1, source_target_pairs={{0,8},{4,12},{8,0},{12,4},{16,24},{20,28},{24,16},{28,20},{1,9},{5... | collective-permute-start | bytes 208904 | tf_op jit(solution)/shard_map/ppermute | solution.py:258
  40.7 11.7 %collective-permute-start.3 = (bf16[384,256]{1,0:T(8,128)(2,1)S(1)}, bf16[384,256]{1,0:T(8,128)(2,1)S(1)}, u32[]{:S(2)}, u32[]{:S(2)}) collective-permute-start(bf16[384,256]{1,0:T(8,128)(2,1)S(1)} %finish.2), channel_id=1, source_target_pairs={{0,1},{1,0},{2,3},{3,2},{4,5},{5,4},{6,7},{7,6},{8,9},{9,8},{10,11... | collective-permute-start | bytes 589832 | tf_op jit(solution)/shard_map/ppermute | solution.py:258
  40.8 11.0 %collective-permute-start.4 = (bf16[384,256]{1,0:T(8,128)(2,1)S(1)}, bf16[384,256]{1,0:T(8,128)(2,1)S(1)}, u32[]{:S(2)}, u32[]{:S(2)}) collective-permute-start(bf16[384,256]{1,0:T(8,128)(2,1)S(1)} %finish.2), channel_id=1, source_target_pairs={{0,2},{1,3},{2,0},{3,1},{4,6},{5,7},{6,4},{7,5},{8,10},{9,11},{10,... | collective-permute-start | bytes 589832 | tf_op jit(solution)/shard_map/ppermute | solution.py:262
  43.6 6.0 %collective-permute-start.8 = (bf16[272,128]{1,0:T(8,128)(2,1)S(1)}, bf16[272,128]{1,0:T(8,128)(2,1)S(1)}, u32[]{:S(2)}, u32[]{:S(2)}) collective-permute-start(bf16[272,128]{1,0:T(8,128)(2,1)S(1)} %maximum_maximum_fusion.3), channel_id=1, source_target_pairs={{0,16},{4,20},{8,24},{12,28},{16,0},{20,4},{24,8},{28,12},{1,17},{... | collective-permute-start | bytes 208904 | tf_op jit(solution)/shard_map/ppermute | solution.py:258
  50.0 5.7 %collective-permute-start.10 = (bf16[384,256]{1,0:T(8,128)(2,1)S(1)}, bf16[384,256]{1,0:T(8,128)(2,1)S(1)}, u32[]{:S(2)}, u32[]{:S(2)}) collective-permute-start(bf16[384,256]{1,0:T(8,128)(2,1)S(1)} %finish.3), channel_id=1, source_target_pairs={{0,2},{1,3},{2,0},{3,1},{4,6},{5,7},{6,4},{7,5},{8,10},{9,11},{10,... | collective-permute-start | bytes 589832 | tf_op jit(solution)/shard_map/ppermute | solution.py:262
  51.6 4.7 %collective-permute-start.9 = (bf16[384,256]{1,0:T(8,128)(2,1)S(1)}, bf16[384,256]{1,0:T(8,128)(2,1)S(1)}, u32[]{:S(2)}, u32[]{:S(2)}) collective-permute-start(bf16[384,256]{1,0:T(8,128)(2,1)S(1)} %finish.3), channel_id=1, source_target_pairs={{0,1},{1,0},{2,3},{3,2},{4,5},{5,4},{6,7},{7,6},{8,9},{9,8},{10,11... | collective-permute-start | bytes 589832 | tf_op jit(solution)/shard_map/ppermute | solution.py:258
  51.8 4.2 %collective-permute-start.5 = (bf16[384,256]{1,0:T(8,128)(2,1)S(1)}, bf16[384,256]{1,0:T(8,128)(2,1)S(1)}, u32[]{:S(2)}, u32[]{:S(2)}) collective-permute-start(bf16[384,256]{1,0:T(8,128)(2,1)S(1)} %collective-permute-done.4), channel_id=1, source_target_pairs={{0,1},{1,0},{2,3},{3,2},{4,5},{5,4},{6,7},{7,6},{8,9},{9,8},{10,11... | collective-permute-start | bytes 589832 | tf_op jit(solution)/shard_map/ppermute | solution.py:258
  55.7 1.4 %collective-permute-start.11 = (bf16[384,256]{1,0:T(8,128)(2,1)S(1)}, bf16[384,256]{1,0:T(8,128)(2,1)S(1)}, u32[]{:S(2)}, u32[]{:S(2)}) collective-permute-start(bf16[384,256]{1,0:T(8,128)(2,1)S(1)} %collective-permute-done.10), channel_id=1, source_target_pairs={{0,1},{1,0},{2,3},{3,2},{4,5},{5,4},{6,7},{7,6},{8,9},{9,8},{10,11... | collective-permute-start | bytes 589832 | tf_op jit(solution)/shard_map/ppermute | solution.py:258
  56.3 6.1 %copy-start.15 = (f32[512]{0:T(512)S(1)}, f32[512]{0:T(512)}, u32[]{:S(2)}) copy-start(f32[512]{0:T(512)} %param.25) | copy-start | bytes 6148
  57.5 2.6 %collective-permute-start.14 = (f32[3,128]{1,0:T(4,128)S(1)}, f32[3,128]{1,0:T(4,128)S(1)}, u32[]{:S(2)}, u32[]{:S(2)}) collective-permute-start(f32[3,128]{1,0:T(4,128)S(1)} %bitcast.40), channel_id=1, source_target_pairs={{0,3},{1,0},{2,1},{3,2},{4,7},{5,4},{6,5},{7,6},{8,11},{9,8},{10,9... | collective-permute-start | bytes 4616 | tf_op jit(solution)/shard_map/ppermute | solution.py:262
  58.8 3.6 %collective-permute-start.13 = (f32[3,128]{1,0:T(4,128)S(1)}, f32[3,128]{1,0:T(4,128)S(1)}, u32[]{:S(2)}, u32[]{:S(2)}) collective-permute-start(f32[3,128]{1,0:T(4,128)S(1)} %bitcast.41), channel_id=1, source_target_pairs={{0,2},{1,3},{2,0},{3,1},{4,6},{5,7},{6,4},{7,5},{8,10},{9,11},{10,... | collective-permute-start | bytes 4616 | tf_op jit(solution)/shard_map/ppermute | solution.py:262
  59.3 3.1 %collective-permute-start.12 = (f32[3,128]{1,0:T(4,128)S(1)}, f32[3,128]{1,0:T(4,128)S(1)}, u32[]{:S(2)}, u32[]{:S(2)}) collective-permute-start(f32[3,128]{1,0:T(4,128)S(1)} %bitcast.42), channel_id=1, source_target_pairs={{0,1},{1,2},{2,3},{3,0},{4,5},{5,6},{6,7},{7,4},{8,9},{9,10},{10,1... | collective-permute-start | bytes 4616 | tf_op jit(solution)/shard_map/ppermute | solution.py:262
  (7 other events, 6.0 us)
